TPU v7x, 32 devices: a whole 2x2x4 slice. The times are simulated.
32 devices in a mesh: ep: 8 (over z, x), tp: 4 (over y, core).
Axes of the slice: x: 2, y: 2, z: 4, core: 2. Of those that a mesh axis runs over, the one named last changes fastest.
Arguments:
- tokens: bfloat16 [256, 2048], P('ep'), may hold values from -24 to 24
- norm_gain: float32 [2048], replicated, may hold values from 0.1 to 1.9
- post_gain: float32 [2048], replicated, may hold values from 0.1 to 1.9
- w_query: bfloat16 [2048, 2048], P(None, 'tp'), may hold values from -0.125 to 0.125
- w_key: bfloat16 [2048, 512], P(None, 'tp'), may hold values from -0.125 to 0.125
- w_value: bfloat16 [2048, 512], P(None, 'tp'), may hold values from -0.125 to 0.125
- w_forget: bfloat16 [2048, 32], replicated, may hold values from -0.25 to 0.25
- w_output: bfloat16 [2048, 2048], P('tp'), may hold values from -0.125 to 0.125
- key_cache: bfloat16 [256, 8, 64, 1024], P('ep', 'tp'), may hold values from -660 to 660
- value_cache: bfloat16 [256, 8, 64, 1024], P('ep', 'tp'), may hold values from -6 to 6
- gate_cache: float32 [256, 32, 1024], P('ep', 'tp'), may hold values from -176.08 to 0, as said below
- lengths: int32 [256], P('ep'), may hold values from 256 to 1024
- routes: int32 [256, 2], P('ep'), may hold values from 0 to 7, all different within a row; in each aligned block of 32 rows (0 to 31, 32 to 63, ...) at most 16 rows name the same one
- route_logits: float32 [256, 2], P('ep'), may hold values from -6 to 6
- w_gate: bfloat16 [8, 2048, 3584], P('ep', None, 'tp'), may hold values from -0.125 to 0.125
- w_up: bfloat16 [8, 2048, 3584], P('ep', None, 'tp'), may hold values from -0.125 to 0.125
- w_down: bfloat16 [8, 3584, 2048], P('ep', 'tp'), may hold values from -0.09375 to 0.09375
Outputs:
- layer_out: bfloat16 [256, 2048], P('ep', 'tp')
Inputs may be any that keep to these rules, and one draw needn't show every extreme that they name: `routes`: each row names 2 different experts. The rows of one index of ep name any one expert at most 16 times, and in every draw some index of ep names some expert exactly 16 times. `gate_cache`: cumulative sums of negative log forget gates along positions: nonincreasing along the last dimension. `lengths`: the new token follows the valid positions of its sequence.
All inputs are finite; a program needn't handle non-finite values.
Results may differ from a plain program's by a relative error of at most 0.011.
Values may be sent and summed in bfloat16 or wider, within the bound.
A program may use at most 64 MiB of HBM per device.

v0:
```python
import functools

import jax
import jax.numpy as jnp
from jax import lax
from jax.experimental import pallas as pl
from jax.experimental.pallas import tpu as pltpu
from jax.sharding import PartitionSpec as P

epsilon = 1e-06
f32 = jnp.float32
bf16 = jnp.bfloat16
MESH = pl.DeviceIdType.MESH
GROUP = 8
LAG = 2


def layer_kernel(
    ep_count,
    tp_count,
    lengths,
    tokens_h,
    gain_h,
    post_h,
    wq_h,
    wk_h,
    wv_h,
    wf_h,
    wo_h,
    key_h,
    value_h,
    gate_h,
    routes_h,
    logits_h,
    wg_h,
    wu_h,
    wd_h,
    out,
    tokens,
    gain,
    post,
    wq,
    wk,
    wv,
    wf,
    wo,
    keys,
    values,
    gates,
    routes,
    logits,
    wg,
    wu,
    wd,
    query_rows,
    forget_rows,
    new_rows,
    fresh_values,
    mixed_rows,
    part_send,
    part_recv,
    pack_send,
    gathered,
    down_send,
    down_recv,
    ret_send,
    ret_recv,
    held,
    small_sem,
    cache_sem,
    part_ss,
    part_rs,
    pack_ss,
    pack_rs,
    fan_ss,
    fan_rs,
    down_ss,
    down_rs,
    ret_ss,
    ret_rs,
):
    ep = lax.axis_index("ep")
    tp = lax.axis_index("tp")
    partner = tp + 1 - 2 * (tp % 2)
    chips = tp_count // 2
    seqs, width = tokens.shape
    heads = gates.shape[1]
    span = gates.shape[2]
    lanes = keys.shape[1]
    own = width // tp_count
    cap = pack_send.shape[1]
    slots = ep_count * cap
    hd = wq.shape[1] // heads
    per_lane = lanes // hd
    group_heads = heads // per_lane

    barrier = pltpu.get_barrier_semaphore()
    for o in range(1, tp_count):
        pl.semaphore_signal(
            barrier, inc=1, device_id={"tp": (tp + o) % tp_count}, device_id_type=MESH
        )

    def greet(k, c):
        pl.semaphore_signal(
            barrier, inc=1, device_id={"ep": (ep + k) % ep_count}, device_id_type=MESH
        )
        return c

    lax.fori_loop(1, ep_count, greet, 0)

    loads = [
        pltpu.make_async_copy(a, b, small_sem.at[i])
        for i, (a, b) in enumerate(
            [
                (tokens_h, tokens),
                (gain_h, gain),
                (wq_h, wq),
                (wk_h, wk),
                (wv_h, wv),
                (wf_h, wf),
                (routes_h, routes),
                (logits_h, logits),
                (post_h, post),
                (wo_h, wo),
                (wg_h, wg),
                (wu_h, wu),
                (wd_h, wd),
            ]
        )
    ]
    for c in loads[:9]:
        c.start()

    def cache_loads(g):
        at = pl.ds(g * GROUP, GROUP)
        return [
            pltpu.make_async_copy(key_h.at[at], keys.at[at], cache_sem.at[0, g]),
            pltpu.make_async_copy(gate_h.at[at], gates.at[at], cache_sem.at[1, g]),
            pltpu.make_async_copy(value_h.at[at], values.at[at], cache_sem.at[2, g]),
        ]

    def start_cache(g, c):
        for copy in cache_loads(g):
            copy.start()
        return c

    lax.fori_loop(0, seqs // GROUP, start_cache, 0)
    for c in loads[9:]:
        c.start()

    loads[0].wait()
    loads[1].wait()
    wide = tokens[...].astype(f32)
    normed = (
        wide * lax.rsqrt(jnp.mean(wide * wide, axis=-1, keepdims=True) + epsilon) * gain[...]
    ).astype(bf16)
    loads[2].wait()
    query = jnp.dot(normed, wq[...], preferred_element_type=f32).astype(bf16).astype(f32)
    query = query * hd ** (-0.5)
    loads[3].wait()
    fresh_key = jnp.dot(normed, wk[...], preferred_element_type=f32).astype(bf16).astype(f32)
    loads[4].wait()
    fresh_values[...] = (
        jnp.dot(normed, wv[...], preferred_element_type=f32).astype(bf16).astype(f32)
    )
    loads[5].wait()
    forget_all = lax.dot_general(
        normed, wf[...], (((1,), (1,)), ((), ())), preferred_element_type=f32
    )
    forget = forget_all[:, 0:heads]
    for j in range(1, tp_count):
        forget = jnp.where(tp == j, forget_all[:, j * heads : (j + 1) * heads], forget)
    forget = jnp.minimum(forget, 0.0) - jnp.log1p(jnp.exp(-jnp.abs(forget)))
    lane_of = lax.broadcasted_iota(jnp.int32, (seqs, lanes), 1) // hd
    for h in range(heads):
        m, place, want = h // per_lane, h % per_lane, h // group_heads
        block = query[:, m * lanes : (m + 1) * lanes]
        if place != want:
            block = pltpu.roll(block, ((want - place) % per_lane) * hd, 1)
        block = jnp.where(lane_of == want, block, 0.0)
        at = pl.ds(h, seqs, stride=heads)
        query_rows[at, :] = block
        new_rows[at, :] = jnp.broadcast_to(
            jnp.sum(block * fresh_key, axis=-1, keepdims=True), (seqs, lanes)
        )
        forget_rows[at, :] = jnp.broadcast_to(forget[:, h : h + 1], (seqs, lanes))

    position = lax.broadcasted_iota(jnp.int32, (heads, span), 1)

    def attend(g, c):
        for copy in cache_loads(g):
            copy.wait()
        for i in range(GROUP):
            b = g * GROUP + i
            at = pl.ds(pl.multiple_of(b * heads, heads), heads)
            length = lengths[b]
            gate = gates[b]
            score = jnp.dot(
                query_rows[at, :].astype(bf16), keys[b], preferred_element_type=f32
            )
            latest = jnp.sum(
                jnp.where(position == length - 1, gate, 0.0), axis=-1, keepdims=True
            )
            fresh = new_rows[at, :][:, 0:1]
            score = score + (latest + forget_rows[at, :][:, 0:1]) - gate
            score = jnp.where(position < length, score, -jnp.inf)
            peak = jnp.maximum(jnp.max(score, axis=-1, keepdims=True), fresh)
            past = jnp.exp(score - peak)
            fresh = jnp.exp(fresh - peak)
            total = jnp.sum(past, axis=-1, keepdims=True) + fresh
            mixed = lax.dot_general(
                past.astype(bf16),
                values[b],
                (((1,), (1,)), ((), ())),
                preferred_element_type=f32,
            )
            mixed_rows[at, :] = (mixed + fresh * fresh_values[pl.ds(b, 1), :]) / total
        return c

    lax.fori_loop(0, seqs // GROUP, attend, 0)

    pieces = []
    for m in range(heads // per_lane):
        piece = jnp.zeros((seqs, lanes), f32)
        for place in range(per_lane):
            h = m * per_lane + place
            want = h // group_heads
            block = mixed_rows[pl.ds(h, seqs, stride=heads), :]
            if place != want:
                block = pltpu.roll(block, ((place - want) % per_lane) * hd, 1)
            piece = jnp.where(lane_of == place, block, piece)
        pieces.append(piece.astype(bf16))
    attended = jnp.concatenate(pieces, axis=1)

    loads[9].wait()
    for j in range(tp_count):
        part_send[j] = jnp.dot(
            attended, wo[:, j * own : (j + 1) * own], preferred_element_type=f32
        ).astype(bf16)
    pl.semaphore_wait(barrier, ep_count - 1 + tp_count - 1)

    def part_copy(o):
        peer = (tp + o) % tp_count
        return pltpu.make_async_remote_copy(
            src_ref=part_send.at[peer],
            dst_ref=part_recv.at[o - 1],
            send_sem=part_ss.at[o - 1],
            recv_sem=part_rs.at[o - 1],
            device_id={"tp": peer},
            device_id_type=MESH,
        )

    part_copies = [part_copy(o) for o in range(1, tp_count)]
    for c in part_copies:
        c.start()
    loads[6].wait()
    loads[7].wait()
    loads[8].wait()
    slot = lax.broadcasted_iota(jnp.int32, (slots, seqs), 0)
    slot_expert, slot_rank = slot // cap, slot % cap
    first = routes[0:1, :] == slot_expert
    second = routes[1:2, :] == slot_expert
    named = jnp.where(jnp.logical_or(first, second), 1.0, 0.0)
    earlier = jnp.where(
        lax.broadcasted_iota(jnp.int32, (seqs, seqs), 0)
        < lax.broadcasted_iota(jnp.int32, (seqs, seqs), 1),
        1.0,
        0.0,
    )
    rank = jnp.dot(named.astype(bf16), earlier.astype(bf16), preferred_element_type=f32)
    chosen = jnp.where(rank == slot_rank.astype(f32), named, 0.0)
    dispatch = chosen.astype(bf16)
    one, two = logits[0:1, :], logits[1:2, :]
    top = jnp.maximum(one, two)
    e_one, e_two = jnp.exp(one - top), jnp.exp(two - top)
    share = jnp.where(first, e_one / (e_one + e_two), e_two / (e_one + e_two))
    weight = (share * chosen).T
    weight_high = weight.astype(bf16)
    weight_low = (weight - weight_high.astype(f32)).astype(bf16)

    columns = pl.ds(pl.multiple_of(tp * own, own), own)
    total = part_send[tp].astype(f32)
    for k, c in enumerate(part_copies):
        c.wait_recv()
        total = total + part_recv[k].astype(f32)
    residual = tokens[:, columns].astype(f32) + total

    packed = jnp.dot(dispatch, residual.astype(bf16), preferred_element_type=f32)
    for e in range(ep_count):
        pack_send[e] = packed[e * cap : (e + 1) * cap].astype(bf16)

    def pack_copy(k):
        return pltpu.make_async_remote_copy(
            src_ref=pack_send.at[(ep + k) % ep_count],
            dst_ref=gathered.at[tp, ep],
            send_sem=pack_ss.at[k],
            recv_sem=pack_rs.at[k],
            device_id={"ep": (ep + k) % ep_count},
            device_id_type=MESH,
        )

    def from_chip(base, d):
        return (base + tp_count - 2 * d) % tp_count

    def fan_copy(way, s):
        relayed = way - (chips - 1)
        block = from_chip(tp, relayed) if way >= chips else tp
        return pltpu.make_async_remote_copy(
            src_ref=gathered.at[block, s],
            dst_ref=gathered.at[block, s],
            send_sem=fan_ss.at[way, s],
            recv_sem=fan_rs.at[way, s],
            device_id={"tp": (tp + 2 * way) % tp_count if 0 < way < chips else partner},
            device_id_type=MESH,
        )

    def start_pack(k, c):
        pack_copy(k).start()
        return c

    lax.fori_loop(1, ep_count, start_pack, 0)
    gathered[tp, ep] = pack_send[ep]

    def fan_out(k, c):
        s = (ep + ep_count - k) % ep_count

        @pl.when(k > 0)
        def _():
            pack_copy(k).wait_recv()

        for way in [*range(1, chips), 0]:
            fan_copy(way, s).start()
        return c

    lax.fori_loop(0, ep_count, fan_out, 0)

    def relay(k, c):
        s = (ep + ep_count - k) % ep_count
        for way in range(1, chips):
            fan_copy(way, s).wait_recv()
            fan_copy(chips - 1 + way, s).start()
        return c

    for c in loads[10:]:
        c.wait()

    def rows_of(block):
        rows = jnp.concatenate(
            [gathered[block, s].astype(f32) for s in range(ep_count)], axis=0
        )
        at = pl.ds(pl.multiple_of(block * own, own), own)
        scaled = (rows * post[:, at]).astype(bf16)
        return (
            jnp.sum(rows * rows, axis=-1, keepdims=True),
            jnp.dot(scaled, wg[at, :], preferred_element_type=f32),
            jnp.dot(scaled, wu[at, :], preferred_element_type=f32),
        )

    def arrive(way):
        def one_source(s, c):
            fan_copy(way, s).wait_recv()
            return c

        lax.fori_loop(0, ep_count, one_source, 0)

    def add(a, b):
        return tuple(x + y for x, y in zip(a, b))

    sums = rows_of(tp)
    lax.fori_loop(0, ep_count, relay, 0)
    arrive(0)
    sums = add(sums, rows_of(partner))
    for d in range(1, chips):
        sums = add(sums, rows_of(from_chip(tp, d)))
    for d in range(1, chips):
        arrive(chips - 1 + d)
        sums = add(sums, rows_of(from_chip(partner, d)))
    squares, gate_act, upper = sums
    scale = lax.rsqrt(squares / width + epsilon)
    gate_act = gate_act * scale
    hidden = (gate_act / (1.0 + jnp.exp(-gate_act)) * (upper * scale)).astype(bf16)

    def down(block):
        at = pl.ds(pl.multiple_of(block * own, own), own)
        return jnp.dot(hidden, wd[:, at], preferred_element_type=f32)

    def down_copy(k, e):
        return pltpu.make_async_remote_copy(
            src_ref=down_send.at[k, e],
            dst_ref=down_recv.at[k, e],
            send_sem=down_ss.at[k, e],
            recv_sem=down_rs.at[k, e],
            device_id={
                "tp": (tp + 2 * (k - chips + 1)) % tp_count if k >= chips else partner
            },
            device_id_type=MESH,
        )

    def turn(k):
        return (ep + 1 + k) % ep_count

    def spread(ref, rows):
        for e in range(ep_count):
            ref[e] = rows[e * cap : (e + 1) * cap].astype(ref.dtype)

    def start_down(way):
        def one(k, c):
            down_copy(way, turn(k)).start()
            return c

        lax.fori_loop(0, ep_count, one, 0)

    def ret_copy(k):
        return pltpu.make_async_remote_copy(
            src_ref=ret_send.at[(ep + k) % ep_count],
            dst_ref=ret_recv.at[ep],
            send_sem=ret_ss.at[k],
            recv_sem=ret_rs.at[k],
            device_id={"ep": (ep + k) % ep_count},
            device_id_type=MESH,
        )

    for d in range(1, chips):
        spread(down_send.at[d - 1], down((partner + 2 * d) % tp_count))
        start_down(d - 1)
    for d in range(1, chips):
        spread(held, down((tp + 2 * d) % tp_count))

        def cross(k, c):
            e = turn(k)
            down_copy(d - 1, e).wait_recv()
            down_send[chips - 1 + d, e] = (
                held[e] + down_recv[d - 1, e].astype(f32)
            ).astype(bf16)
            down_copy(chips - 1 + d, e).start()
            return c

        lax.fori_loop(0, ep_count, cross, 0)
    spread(down_send.at[chips - 1], down(partner))
    start_down(chips - 1)
    spread(held, down(tp))

    def give_back(k, c):
        e = turn(k)
        total = held[e]
        for way in range(chips - 1, 2 * chips - 1):
            down_copy(way, e).wait_recv()
            total = total + down_recv[way, e].astype(f32)

        @pl.when(k < ep_count - 1)
        def _():
            ret_send[e] = total.astype(bf16)
            ret_copy(k + 1).start()

        @pl.when(k == ep_count - 1)
        def _():
            ret_recv[e] = total.astype(bf16)

        return c

    lax.fori_loop(0, ep_count, give_back, 0)

    def wait_ret(k, c):
        ret_copy(k).wait_recv()
        return c

    lax.fori_loop(1, ep_count, wait_ret, 0)
    returned = jnp.concatenate(
        [ret_recv[e].astype(f32) for e in range(ep_count)], axis=0
    ).astype(bf16)
    mix = jnp.dot(weight_high, returned, preferred_element_type=f32) + jnp.dot(
        weight_low, returned, preferred_element_type=f32
    )
    out[...] = (residual + mix).astype(bf16)

    for c in part_copies:
        c.wait_send()

    def finish(k, c):
        pack_copy(k).wait_send()
        ret_copy(k).wait_send()
        return c

    lax.fori_loop(1, ep_count, finish, 0)

    def finish_fan(s, c):
        for way in range(2 * chips - 1):
            fan_copy(way, s).wait_send()
            down_copy(way, s).wait_send()
        return c

    lax.fori_loop(0, ep_count, finish_fan, 0)


def body(
    tokens,
    norm_gain,
    post_gain,
    w_query,
    w_key,
    w_value,
    w_forget,
    w_output,
    key_cache,
    value_cache,
    gate_cache,
    lengths,
    routes,
    route_logits,
    w_gate,
    w_up,
    w_down,
):
    ep_count = lax.axis_size("ep")
    tp_count = lax.axis_size("tp")
    ways = tp_count - 1
    seqs, width = tokens.shape
    heads, span = gate_cache.shape[1:]
    own = width // tp_count
    cap = 2 * seqs * routes.shape[1] // ep_count
    lanes = key_cache.shape[1] * key_cache.shape[2]
    hbm = [
        tokens,
        norm_gain.reshape(1, width),
        post_gain.reshape(1, width),
        w_query,
        w_key,
        w_value,
        w_forget.T,
        w_output,
        key_cache.reshape(seqs, lanes, span),
        value_cache.reshape(seqs, lanes, span),
        gate_cache,
        routes.T,
        route_logits.T,
        w_gate.reshape(w_gate.shape[1:]),
        w_up.reshape(w_up.shape[1:]),
        w_down.reshape(w_down.shape[1:]),
    ]
    dma = pltpu.SemaphoreType.DMA
    scratch = [pltpu.VMEM(a.shape, a.dtype) for a in hbm] + [
        pltpu.VMEM((seqs * heads, lanes), f32),
        pltpu.VMEM((seqs * heads, lanes), f32),
        pltpu.VMEM((seqs * heads, lanes), f32),
        pltpu.VMEM((seqs, lanes), f32),
        pltpu.VMEM((seqs * heads, lanes), f32),
        pltpu.VMEM((tp_count, seqs, own), bf16),
        pltpu.VMEM((ways, seqs, own), bf16),
        pltpu.VMEM((ep_count, cap, own), bf16),
        pltpu.VMEM((tp_count, ep_count, cap, own), bf16),
        pltpu.VMEM((ways, ep_count, cap, own), bf16),
        pltpu.VMEM((ways, ep_count, cap, own), bf16),
        pltpu.VMEM((ep_count, cap, own), bf16),
        pltpu.VMEM((ep_count, cap, own), bf16),
        pltpu.VMEM((ep_count, cap, own), f32),
        dma((13,)),
        dma((3, seqs // GROUP)),
        dma((ways,)),
        dma((ways,)),
        dma((ep_count,)),
        dma((ep_count,)),
        dma((ways, ep_count)),
        dma((ways, ep_count)),
        dma((ways, ep_count)),
        dma((ways, ep_count)),
        dma((ep_count,)),
        dma((ep_count,)),
    ]
    return pl.pallas_call(
        functools.partial(layer_kernel, ep_count, tp_count),
        out_shape=jax.ShapeDtypeStruct((seqs, own), bf16),
        in_specs=[pl.BlockSpec(memory_space=pltpu.SMEM)]
        + [pl.BlockSpec(memory_space=pl.ANY)] * len(hbm),
        out_specs=pl.BlockSpec(memory_space=pltpu.VMEM),
        scratch_shapes=scratch,
        compiler_params=pltpu.CompilerParams(
            collective_id=0, has_side_effects=True, vmem_limit_bytes=60 * 1024 * 1024
        ),
    )(lengths, *hbm)


def solution(mesh):
    in_specs = (
        P("ep", None),
        P(),
        P(),
        P(None, "tp"),
        P(None, "tp"),
        P(None, "tp"),
        P(),
        P("tp", None),
        P("ep", "tp", None, None),
        P("ep", "tp", None, None),
        P("ep", "tp", None),
        P("ep"),
        P("ep", None),
        P("ep", None),
        P("ep", None, "tp"),
        P("ep", None, "tp"),
        P("ep", "tp", None),
    )
    out_specs = P("ep", "tp")
    return jax.shard_map(body, mesh=mesh, in_specs=in_specs, out_specs=out_specs, check_vma=False)
```

profile of v0, /device:TPU:0, one launch (start us, length us, event | category | flops | bytes accessed | tf_op | source)
XLA Modules:
  0.0 41.6 jit_solution(9212571325485818113)
XLA Ops:
  0.0 40.3 %shard_map.163 = bf16[32,512]{1,0:T(8,128)(2,1)} custom-call(s32[32]{0:T(128)} %lengths.1, bf16[32,2048]{1,0:T(8,128)(2,1)} %tokens_h.1, f32[1,2048]{1,0:T(1,128)} %bitcast.16, f32[1,2048]{1,0:T(1,128)} %bitcast.17, bf16[2048,512]{1,0:T(8,128)(2,1)} %wq_h.1, bf16[2048,128]{1,0:T(8,128)(2,1)} %wk_h.1, bf16[2048,128]{1,0:T(8,128)(2,1)} %wv_h.1, ...), custom_call_target="tpu_custom_call" | custom-call | tf_op jit(solution)/shard_map/pallas_call | solution.py:569
  40.3 1.4 %copy.19 = bf16[32,512]{1,0:T(8,128)(2,1)} copy(bf16[32,512]{1,0:T(8,128)(2,1)} %shard_map.163) | data formatting | bytes 65536
where the time goes:
time: 41.8 us; the launch traced here: 41.6 us
  Pallas kernels  40.3 us (96%)
  local copies, waits for them, and re-layouts  1.38 us (3%)
    pallas_call x1, Pallas kernels, body(): pl.pallas_call(functools.partial(layer_kernel, ep_count, tp_count), out_s...  40.3 us
    unnamed x1, local copies, waits for them, and re-layouts  1.38 us

commit v1 on v0

--- a/solution.py
+++ b/solution.py
@@ -12,7 +12,7 @@
 bf16 = jnp.bfloat16
 MESH = pl.DeviceIdType.MESH
 GROUP = 8
-LAG = 2
+AHEAD = 2
 
 
 def layer_kernel(
@@ -40,8 +40,7 @@
     gain,
     post,
     wq,
-    wk,
-    wv,
+    wkv,
     wf,
     wo,
     keys,
@@ -57,6 +56,10 @@
     new_rows,
     fresh_values,
     mixed_rows,
+    scores,
+    probs,
+    fresh_rows,
+    total_rows,
     part_send,
     part_recv,
     pack_send,
@@ -67,6 +70,7 @@
     ret_recv,
     held,
     small_sem,
+    pair_sem,
     cache_sem,
     part_ss,
     part_rs,
@@ -74,8 +78,10 @@
     pack_rs,
     fan_ss,
     fan_rs,
+    fan_all,
     down_ss,
     down_rs,
+    down_all,
     ret_ss,
     ret_rs,
 ):
@@ -108,6 +114,13 @@
 
     lax.fori_loop(1, ep_count, greet, 0)
 
+    beside = len(wkv.shape) == 2
+    pair_loads = [
+        pltpu.make_async_copy(
+            a, wkv.at[:, pl.ds(i * lanes, lanes)] if beside else wkv.at[i], pair_sem.at[0]
+        )
+        for i, a in enumerate([wk_h, wv_h])
+    ]
     loads = [
         pltpu.make_async_copy(a, b, small_sem.at[i])
         for i, (a, b) in enumerate(
@@ -115,8 +128,6 @@
                 (tokens_h, tokens),
                 (gain_h, gain),
                 (wq_h, wq),
-                (wk_h, wk),
-                (wv_h, wv),
                 (wf_h, wf),
                 (routes_h, routes),
                 (logits_h, logits),
@@ -128,42 +139,49 @@
             ]
         )
     ]
-    for c in loads[:9]:
+    for c in [*loads[:3], *pair_loads, *loads[3:7]]:
         c.start()
 
-    def cache_loads(g):
+    groups = seqs // GROUP
+
+    def cache_load(kind, g):
         at = pl.ds(g * GROUP, GROUP)
-        return [
-            pltpu.make_async_copy(key_h.at[at], keys.at[at], cache_sem.at[0, g]),
-            pltpu.make_async_copy(gate_h.at[at], gates.at[at], cache_sem.at[1, g]),
-            pltpu.make_async_copy(value_h.at[at], values.at[at], cache_sem.at[2, g]),
-        ]
-
-    def start_cache(g, c):
-        for copy in cache_loads(g):
-            copy.start()
-        return c
-
-    lax.fori_loop(0, seqs // GROUP, start_cache, 0)
-    for c in loads[9:]:
-        c.start()
+        a, b = ((key_h, keys), (gate_h, gates), (value_h, values))[kind]
+        return pltpu.make_async_copy(a.at[at], b.at[at], cache_sem.at[kind, g])
+
+    def start_stage(g):
+        def pick(ok, start):
+            if isinstance(g, int):
+                if ok:
+                    start()
+            else:
+                pl.when(ok)(start)
+
+        pick(g < groups, lambda: [cache_load(kind, g).start() for kind in (0, 1)] and None)
+        pick((g > 0) & (g <= groups), lambda: cache_load(2, g - 1).start())
+        for i in range(4):
+            pick(g == groups + i, loads[7 + i].start)
 
     loads[0].wait()
     loads[1].wait()
+    start_stage(0)
     wide = tokens[...].astype(f32)
     normed = (
         wide * lax.rsqrt(jnp.mean(wide * wide, axis=-1, keepdims=True) + epsilon) * gain[...]
     ).astype(bf16)
-    loads[2].wait()
+    for c in loads[2:4]:
+        c.wait()
+    pltpu.make_async_copy(wkv, wkv, pair_sem.at[0]).wait()
+    start_stage(1)
     query = jnp.dot(normed, wq[...], preferred_element_type=f32).astype(bf16).astype(f32)
     query = query * hd ** (-0.5)
-    loads[3].wait()
-    fresh_key = jnp.dot(normed, wk[...], preferred_element_type=f32).astype(bf16).astype(f32)
-    loads[4].wait()
-    fresh_values[...] = (
-        jnp.dot(normed, wv[...], preferred_element_type=f32).astype(bf16).astype(f32)
-    )
-    loads[5].wait()
+    if beside:
+        fresh_pair = jnp.dot(normed, wkv[...], preferred_element_type=f32)
+        fresh_pair = fresh_pair[:, :lanes], fresh_pair[:, lanes:]
+    else:
+        fresh_pair = [jnp.dot(normed, wkv[i], preferred_element_type=f32) for i in range(2)]
+    fresh_key, fresh_value = [a.astype(bf16).astype(f32) for a in fresh_pair]
+    fresh_values[...] = fresh_value
     forget_all = lax.dot_general(
         normed, wf[...], (((1,), (1,)), ((), ())), preferred_element_type=f32
     )
@@ -187,37 +205,76 @@
 
     position = lax.broadcasted_iota(jnp.int32, (heads, span), 1)
 
-    def attend(g, c):
-        for copy in cache_loads(g):
-            copy.wait()
+    def rows_at(b):
+        return pl.ds(pl.multiple_of(b * heads, heads), heads)
+
+    def score(g):
         for i in range(GROUP):
             b = g * GROUP + i
-            at = pl.ds(pl.multiple_of(b * heads, heads), heads)
+            scores[g % 2, i] = jnp.dot(
+                query_rows[rows_at(b), :].astype(bf16), keys[b], preferred_element_type=f32
+            )
+
+    def soften(g):
+        for i in range(GROUP):
+            b = g * GROUP + i
             length = lengths[b]
             gate = gates[b]
-            score = jnp.dot(
-                query_rows[at, :].astype(bf16), keys[b], preferred_element_type=f32
-            )
             latest = jnp.sum(
                 jnp.where(position == length - 1, gate, 0.0), axis=-1, keepdims=True
             )
-            fresh = new_rows[at, :][:, 0:1]
-            score = score + (latest + forget_rows[at, :][:, 0:1]) - gate
-            score = jnp.where(position < length, score, -jnp.inf)
-            peak = jnp.maximum(jnp.max(score, axis=-1, keepdims=True), fresh)
-            past = jnp.exp(score - peak)
+            fresh = new_rows[rows_at(b), :][:, 0:1]
+            past = scores[g % 2, i] + (latest + forget_rows[rows_at(b), :][:, 0:1]) - gate
+            past = jnp.where(position < length, past, -jnp.inf)
+            peak = jnp.maximum(jnp.max(past, axis=-1, keepdims=True), fresh)
+            past = jnp.exp(past - peak)
             fresh = jnp.exp(fresh - peak)
             total = jnp.sum(past, axis=-1, keepdims=True) + fresh
+            probs[g % 2, i] = past.astype(bf16)
+            fresh_rows[g % 2, i] = jnp.broadcast_to(fresh, (heads, lanes))
+            total_rows[g % 2, i] = jnp.broadcast_to(total, (heads, lanes))
+
+    def blend(g):
+        for i in range(GROUP):
+            b = g * GROUP + i
             mixed = lax.dot_general(
-                past.astype(bf16),
+                probs[g % 2, i],
                 values[b],
                 (((1,), (1,)), ((), ())),
                 preferred_element_type=f32,
             )
-            mixed_rows[at, :] = (mixed + fresh * fresh_values[pl.ds(b, 1), :]) / total
+            mixed_rows[rows_at(b), :] = (
+                mixed + fresh_rows[g % 2, i] * fresh_values[pl.ds(b, 1), :]
+            ) / total_rows[g % 2, i]
+
+    def arrived(kinds, g):
+        for kind in kinds:
+            cache_load(kind, g).wait()
+
+    def attend(g, c):
+        arrived((0, 1), g)
+        arrived((2,), g - 2)
+        start_stage(g + AHEAD)
+        blend(g - 2)
+        soften(g - 1)
+        score(g)
         return c
 
-    lax.fori_loop(0, seqs // GROUP, attend, 0)
+    arrived((0, 1), 0)
+    start_stage(AHEAD)
+    score(0)
+    arrived((0, 1), 1)
+    start_stage(AHEAD + 1)
+    soften(0)
+    score(1)
+    lax.fori_loop(2, groups, attend, 0)
+    for g in range(groups + AHEAD, groups + 4):
+        start_stage(g)
+    arrived((2,), groups - 2)
+    blend(groups - 2)
+    soften(groups - 1)
+    arrived((2,), groups - 1)
+    blend(groups - 1)
 
     pieces = []
     for m in range(heads // per_lane):
@@ -232,20 +289,23 @@
         pieces.append(piece.astype(bf16))
     attended = jnp.concatenate(pieces, axis=1)
 
-    loads[9].wait()
+    loads[7].wait()
     for j in range(tp_count):
         part_send[j] = jnp.dot(
             attended, wo[:, j * own : (j + 1) * own], preferred_element_type=f32
         ).astype(bf16)
     pl.semaphore_wait(barrier, ep_count - 1 + tp_count - 1)
 
+    def received(ref, sem):
+        pltpu.make_async_copy(ref, ref, sem).wait()
+
     def part_copy(o):
         peer = (tp + o) % tp_count
         return pltpu.make_async_remote_copy(
             src_ref=part_send.at[peer],
             dst_ref=part_recv.at[o - 1],
-            send_sem=part_ss.at[o - 1],
-            recv_sem=part_rs.at[o - 1],
+            send_sem=part_ss.at[0],
+            recv_sem=part_rs.at[0],
             device_id={"tp": peer},
             device_id_type=MESH,
         )
@@ -253,9 +313,8 @@
     part_copies = [part_copy(o) for o in range(1, tp_count)]
     for c in part_copies:
         c.start()
-    loads[6].wait()
-    loads[7].wait()
-    loads[8].wait()
+    for c in loads[4:7]:
+        c.wait()
     slot = lax.broadcasted_iota(jnp.int32, (slots, seqs), 0)
     slot_expert, slot_rank = slot // cap, slot % cap
     first = routes[0:1, :] == slot_expert
@@ -280,8 +339,8 @@
 
     columns = pl.ds(pl.multiple_of(tp * own, own), own)
     total = part_send[tp].astype(f32)
-    for k, c in enumerate(part_copies):
-        c.wait_recv()
+    received(part_recv, part_rs.at[0])
+    for k in range(tp_count - 1):
         total = total + part_recv[k].astype(f32)
     residual = tokens[:, columns].astype(f32) + total
 
@@ -293,7 +352,7 @@
         return pltpu.make_async_remote_copy(
             src_ref=pack_send.at[(ep + k) % ep_count],
             dst_ref=gathered.at[tp, ep],
-            send_sem=pack_ss.at[k],
+            send_sem=pack_ss.at[0],
             recv_sem=pack_rs.at[k],
             device_id={"ep": (ep + k) % ep_count},
             device_id_type=MESH,
@@ -303,13 +362,13 @@
         return (base + tp_count - 2 * d) % tp_count
 
     def fan_copy(way, s):
-        relayed = way - (chips - 1)
-        block = from_chip(tp, relayed) if way >= chips else tp
+        relayed = way - (chips - 1) if way >= chips else 0
+        block = from_chip(tp, relayed) if relayed else tp
         return pltpu.make_async_remote_copy(
             src_ref=gathered.at[block, s],
             dst_ref=gathered.at[block, s],
-            send_sem=fan_ss.at[way, s],
-            recv_sem=fan_rs.at[way, s],
+            send_sem=fan_ss.at[0],
+            recv_sem=fan_rs.at[way - 1, s] if 0 < way < chips else fan_all.at[max(0, relayed)],
             device_id={"tp": (tp + 2 * way) % tp_count if 0 < way < chips else partner},
             device_id_type=MESH,
         )
@@ -341,7 +400,7 @@
             fan_copy(chips - 1 + way, s).start()
         return c
 
-    for c in loads[10:]:
+    for c in loads[8:]:
         c.wait()
 
     def rows_of(block):
@@ -356,12 +415,8 @@
             jnp.dot(scaled, wu[at, :], preferred_element_type=f32),
         )
 
-    def arrive(way):
-        def one_source(s, c):
-            fan_copy(way, s).wait_recv()
-            return c
-
-        lax.fori_loop(0, ep_count, one_source, 0)
+    def arrive(relayed):
+        received(gathered.at[0], fan_all.at[relayed])
 
     def add(a, b):
         return tuple(x + y for x, y in zip(a, b))
@@ -373,7 +428,7 @@
     for d in range(1, chips):
         sums = add(sums, rows_of(from_chip(tp, d)))
     for d in range(1, chips):
-        arrive(chips - 1 + d)
+        arrive(d)
         sums = add(sums, rows_of(from_chip(partner, d)))
     squares, gate_act, upper = sums
     scale = lax.rsqrt(squares / width + epsilon)
@@ -388,8 +443,8 @@
         return pltpu.make_async_remote_copy(
             src_ref=down_send.at[k, e],
             dst_ref=down_recv.at[k, e],
-            send_sem=down_ss.at[k, e],
-            recv_sem=down_rs.at[k, e],
+            send_sem=down_ss.at[0],
+            recv_sem=down_rs.at[k, e] if k < chips - 1 else down_all.at[e],
             device_id={
                 "tp": (tp + 2 * (k - chips + 1)) % tp_count if k >= chips else partner
             },
@@ -414,8 +469,8 @@
         return pltpu.make_async_remote_copy(
             src_ref=ret_send.at[(ep + k) % ep_count],
             dst_ref=ret_recv.at[ep],
-            send_sem=ret_ss.at[k],
-            recv_sem=ret_rs.at[k],
+            send_sem=ret_ss.at[0],
+            recv_sem=ret_rs.at[0],
             device_id={"ep": (ep + k) % ep_count},
             device_id_type=MESH,
         )
@@ -443,8 +498,8 @@
     def give_back(k, c):
         e = turn(k)
         total = held[e]
+        received(down_recv.at[pl.ds(chips - 1, chips), e], down_all.at[e])
         for way in range(chips - 1, 2 * chips - 1):
-            down_copy(way, e).wait_recv()
             total = total + down_recv[way, e].astype(f32)
 
         @pl.when(k < ep_count - 1)
@@ -460,11 +515,7 @@
 
     lax.fori_loop(0, ep_count, give_back, 0)
 
-    def wait_ret(k, c):
-        ret_copy(k).wait_recv()
-        return c
-
-    lax.fori_loop(1, ep_count, wait_ret, 0)
+    received(ret_recv.at[pl.ds(0, ep_count - 1)], ret_rs.at[0])
     returned = jnp.concatenate(
         [ret_recv[e].astype(f32) for e in range(ep_count)], axis=0
     ).astype(bf16)
@@ -473,23 +524,11 @@
     )
     out[...] = (residual + mix).astype(bf16)
 
-    for c in part_copies:
-        c.wait_send()
-
-    def finish(k, c):
-        pack_copy(k).wait_send()
-        ret_copy(k).wait_send()
-        return c
-
-    lax.fori_loop(1, ep_count, finish, 0)
-
-    def finish_fan(s, c):
-        for way in range(2 * chips - 1):
-            fan_copy(way, s).wait_send()
-            down_copy(way, s).wait_send()
-        return c
-
-    lax.fori_loop(0, ep_count, finish_fan, 0)
+    received(part_recv, part_ss.at[0])
+    received(ret_recv.at[pl.ds(0, ep_count - 1)], pack_ss.at[0])
+    received(ret_recv.at[pl.ds(0, ep_count - 1)], ret_ss.at[0])
+    received(down_recv, fan_ss.at[0])
+    received(down_recv, down_ss.at[0])
 
 
 def body(
@@ -538,12 +577,19 @@
         w_down.reshape(w_down.shape[1:]),
     ]
     dma = pltpu.SemaphoreType.DMA
-    scratch = [pltpu.VMEM(a.shape, a.dtype) for a in hbm] + [
+    pair = (width, 2 * lanes) if lanes % 128 == 0 else (2, width, lanes)
+    scratch = [
+        pltpu.VMEM(pair if a is w_key else a.shape, a.dtype) for a in hbm if a is not w_value
+    ] + [
         pltpu.VMEM((seqs * heads, lanes), f32),
         pltpu.VMEM((seqs * heads, lanes), f32),
         pltpu.VMEM((seqs * heads, lanes), f32),
         pltpu.VMEM((seqs, lanes), f32),
         pltpu.VMEM((seqs * heads, lanes), f32),
+        pltpu.VMEM((2, GROUP, heads, span), f32),
+        pltpu.VMEM((2, GROUP, heads, span), bf16),
+        pltpu.VMEM((2, GROUP, heads, lanes), f32),
+        pltpu.VMEM((2, GROUP, heads, lanes), f32),
         pltpu.VMEM((tp_count, seqs, own), bf16),
         pltpu.VMEM((ways, seqs, own), bf16),
         pltpu.VMEM((ep_count, cap, own), bf16),
@@ -553,30 +599,33 @@
         pltpu.VMEM((ep_count, cap, own), bf16),
         pltpu.VMEM((ep_count, cap, own), bf16),
         pltpu.VMEM((ep_count, cap, own), f32),
-        dma((13,)),
+        dma((11,)),
+        dma((1,)),
         dma((3, seqs // GROUP)),
-        dma((ways,)),
-        dma((ways,)),
+        dma((1,)),
+        dma((1,)),
+        dma((1,)),
         dma((ep_count,)),
+        dma((1,)),
+        dma((tp_count // 2 - 1, ep_count)),
+        dma((tp_count // 2,)),
+        dma((1,)),
+        dma((tp_count // 2 - 1, ep_count)),
         dma((ep_count,)),
-        dma((ways, ep_count)),
-        dma((ways, ep_count)),
-        dma((ways, ep_count)),
-        dma((ways, ep_count)),
-        dma((ep_count,)),
-        dma((ep_count,)),
+        dma((1,)),
+        dma((1,)),
     ]
     return pl.pallas_call(
         functools.partial(layer_kernel, ep_count, tp_count),
-        out_shape=jax.ShapeDtypeStruct((seqs, own), bf16),
+        out_shape=pltpu.VMEM((seqs, own), bf16),
         in_specs=[pl.BlockSpec(memory_space=pltpu.SMEM)]
         + [pl.BlockSpec(memory_space=pl.ANY)] * len(hbm),
         out_specs=pl.BlockSpec(memory_space=pltpu.VMEM),
         scratch_shapes=scratch,
         compiler_params=pltpu.CompilerParams(
-            collective_id=0, has_side_effects=True, vmem_limit_bytes=60 * 1024 * 1024
+            collective_id=0, has_side_effects=True, vmem_limit_bytes=48 * 1024 * 1024
         ),
-    )(lengths, *hbm)
+    )(*[pltpu.with_memory_space_constraint(a, pltpu.HBM) for a in [lengths, *hbm]])
 
 
 def solution(mesh):

time: 41.8 us -> 36.9 us (0.88)
  Pallas kernels: 40.3 us -> 36.1 us
  local copies, waits for them, and re-layouts: 1.38 us -> 0.62 us
    pallas_call x1, Pallas kernels: 40.3 us -> 36.1 us  [body(): pl.pallas_call(functools.partial(layer_kernel, ep_count, tp_count), out_s...]
    unnamed x1, local copies, waits for them, and re-layouts: 1.38 us -> 0.62 us
where the time goes in v1:
time: 36.9 us; the launch traced here: 36.7 us
  Pallas kernels  36.1 us (98%)
  local copies, waits for them, and re-layouts  0.62 us (2%)
    pallas_call x1, Pallas kernels, body(): pl.pallas_call(functools.partial(layer_kernel, ep_count, tp_count), out_s...  36.1 us

profile of v1, /device:TPU:0, one launch (start us, length us, event | category | flops | bytes accessed | tf_op | source)
XLA Modules:
  0.0 36.7 jit_solution(17959636550560074655)
XLA Ops:
  0.0 36.1 %shard_map.163 = bf16[32,512]{1,0:T(8,128)(2,1)S(1)} custom-call(s32[32]{0:T(128)} %lengths.1, bf16[32,2048]{1,0:T(8,128)(2,1)} %tokens_h.1, f32[1,2048]{1,0:T(1,128)} %bitcast.16, f32[1,2048]{1,0:T(1,128)} %bitcast.17, bf16[2048,512]{1,0:T(8,128)(2,1)} %wq_h.1, bf16[2048,128]{1,0:T(8,128)(2,1)} %wk_h.1, bf16[2048,128]{1,0:T(8,128)(2,1)} %wv_h.1, ...), custom_call_target="tpu_custom_call" | custom-call | tf_op jit(solution)/shard_map/pallas_call | solution.py:618
  36.1 0.6 %copy.19 = bf16[32,512]{1,0:T(8,128)(2,1)} copy(bf16[32,512]{1,0:T(8,128)(2,1)S(1)} %shard_map.163) | data formatting | bytes 65536

commit v2 on v1

--- a/solution.py
+++ b/solution.py
@@ -12,7 +12,7 @@
 bf16 = jnp.bfloat16
 MESH = pl.DeviceIdType.MESH
 GROUP = 8
-AHEAD = 2
+AHEAD = 4
 
 
 def layer_kernel(
@@ -48,12 +48,11 @@
     gates,
     routes,
     logits,
-    wg,
-    wu,
+    wgu,
     wd,
     query_rows,
     forget_rows,
-    new_rows,
+    fresh_keys,
     fresh_values,
     mixed_rows,
     scores,
@@ -121,6 +120,14 @@
         )
         for i, a in enumerate([wk_h, wv_h])
     ]
+    inner = wg_h.shape[1]
+    joined = len(wgu.shape) == 2
+    expert_loads = [
+        pltpu.make_async_copy(
+            a, wgu.at[:, pl.ds(i * inner, inner)] if joined else wgu.at[i], pair_sem.at[1]
+        )
+        for i, a in enumerate([wg_h, wu_h])
+    ]
     loads = [
         pltpu.make_async_copy(a, b, small_sem.at[i])
         for i, (a, b) in enumerate(
@@ -133,8 +140,6 @@
                 (logits_h, logits),
                 (post_h, post),
                 (wo_h, wo),
-                (wg_h, wg),
-                (wu_h, wu),
                 (wd_h, wd),
             ]
         )
@@ -159,12 +164,13 @@
 
         pick(g < groups, lambda: [cache_load(kind, g).start() for kind in (0, 1)] and None)
         pick((g > 0) & (g <= groups), lambda: cache_load(2, g - 1).start())
-        for i in range(4):
-            pick(g == groups + i, loads[7 + i].start)
-
+        for i, load in enumerate([loads[7], *expert_loads, loads[8]]):
+            pick(g == groups + i, load.start)
+
+    start_stage(0)
     loads[0].wait()
     loads[1].wait()
-    start_stage(0)
+    start_stage(1)
     wide = tokens[...].astype(f32)
     normed = (
         wide * lax.rsqrt(jnp.mean(wide * wide, axis=-1, keepdims=True) + epsilon) * gain[...]
@@ -172,7 +178,8 @@
     for c in loads[2:4]:
         c.wait()
     pltpu.make_async_copy(wkv, wkv, pair_sem.at[0]).wait()
-    start_stage(1)
+    start_stage(2)
+    start_stage(3)
     query = jnp.dot(normed, wq[...], preferred_element_type=f32).astype(bf16).astype(f32)
     query = query * hd ** (-0.5)
     if beside:
@@ -182,6 +189,7 @@
         fresh_pair = [jnp.dot(normed, wkv[i], preferred_element_type=f32) for i in range(2)]
     fresh_key, fresh_value = [a.astype(bf16).astype(f32) for a in fresh_pair]
     fresh_values[...] = fresh_value
+    fresh_keys[...] = fresh_key
     forget_all = lax.dot_general(
         normed, wf[...], (((1,), (1,)), ((), ())), preferred_element_type=f32
     )
@@ -198,9 +206,6 @@
         block = jnp.where(lane_of == want, block, 0.0)
         at = pl.ds(h, seqs, stride=heads)
         query_rows[at, :] = block
-        new_rows[at, :] = jnp.broadcast_to(
-            jnp.sum(block * fresh_key, axis=-1, keepdims=True), (seqs, lanes)
-        )
         forget_rows[at, :] = jnp.broadcast_to(forget[:, h : h + 1], (seqs, lanes))
 
     position = lax.broadcasted_iota(jnp.int32, (heads, span), 1)
@@ -223,7 +228,9 @@
             latest = jnp.sum(
                 jnp.where(position == length - 1, gate, 0.0), axis=-1, keepdims=True
             )
-            fresh = new_rows[rows_at(b), :][:, 0:1]
+            fresh = jnp.sum(
+                query_rows[rows_at(b), :] * fresh_keys[pl.ds(b, 1), :], axis=-1, keepdims=True
+            )
             past = scores[g % 2, i] + (latest + forget_rows[rows_at(b), :][:, 0:1]) - gate
             past = jnp.where(position < length, past, -jnp.inf)
             peak = jnp.maximum(jnp.max(past, axis=-1, keepdims=True), fresh)
@@ -290,17 +297,19 @@
     attended = jnp.concatenate(pieces, axis=1)
 
     loads[7].wait()
-    for j in range(tp_count):
-        part_send[j] = jnp.dot(
-            attended, wo[:, j * own : (j + 1) * own], preferred_element_type=f32
+    pl.semaphore_wait(barrier, ep_count - 1 + tp_count - 1)
+
+    def project(peer):
+        at = pl.ds(pl.multiple_of(peer * own, own), own)
+        part_send[peer] = jnp.dot(
+            attended, wo[:, at], preferred_element_type=f32
         ).astype(bf16)
-    pl.semaphore_wait(barrier, ep_count - 1 + tp_count - 1)
 
     def received(ref, sem):
         pltpu.make_async_copy(ref, ref, sem).wait()
 
-    def part_copy(o):
-        peer = (tp + o) % tp_count
+    def part_copy(peer):
+        o = (peer + tp_count - tp) % tp_count
         return pltpu.make_async_remote_copy(
             src_ref=part_send.at[peer],
             dst_ref=part_recv.at[o - 1],
@@ -310,9 +319,13 @@
             device_id_type=MESH,
         )
 
-    part_copies = [part_copy(o) for o in range(1, tp_count)]
-    for c in part_copies:
-        c.start()
+    for d in [*range(1, chips), 0]:
+        for base in (tp, partner):
+            if d or base is partner:
+                peer = (base + 2 * d) % tp_count
+                project(peer)
+                part_copy(peer).start()
+    project(tp)
     for c in loads[4:7]:
         c.wait()
     slot = lax.broadcasted_iota(jnp.int32, (slots, seqs), 0)
@@ -336,6 +349,7 @@
     weight = (share * chosen).T
     weight_high = weight.astype(bf16)
     weight_low = (weight - weight_high.astype(f32)).astype(bf16)
+    weight_both = jnp.concatenate([weight_high, weight_low], axis=0)
 
     columns = pl.ds(pl.multiple_of(tp * own, own), own)
     total = part_send[tp].astype(f32)
@@ -348,13 +362,26 @@
     for e in range(ep_count):
         pack_send[e] = packed[e * cap : (e + 1) * cap].astype(bf16)
 
+    paired = ep_count & (ep_count - 1) == 0
+
+    def across(k):
+        if not paired:
+            return (ep + k) % ep_count
+        e, bit = 0, 1
+        while bit < ep_count:
+            e, bit = e + (ep // bit + k // bit) % 2 * bit, 2 * bit
+        return e
+
+    def source(k):
+        return across(k) if paired else (ep + ep_count - k) % ep_count
+
     def pack_copy(k):
         return pltpu.make_async_remote_copy(
-            src_ref=pack_send.at[(ep + k) % ep_count],
+            src_ref=pack_send.at[across(k)],
             dst_ref=gathered.at[tp, ep],
             send_sem=pack_ss.at[0],
             recv_sem=pack_rs.at[k],
-            device_id={"ep": (ep + k) % ep_count},
+            device_id={"ep": across(k)},
             device_id_type=MESH,
         )
 
@@ -381,7 +408,7 @@
     gathered[tp, ep] = pack_send[ep]
 
     def fan_out(k, c):
-        s = (ep + ep_count - k) % ep_count
+        s = source(k)
 
         @pl.when(k > 0)
         def _():
@@ -394,14 +421,14 @@
     lax.fori_loop(0, ep_count, fan_out, 0)
 
     def relay(k, c):
-        s = (ep + ep_count - k) % ep_count
+        s = source(k)
         for way in range(1, chips):
             fan_copy(way, s).wait_recv()
             fan_copy(chips - 1 + way, s).start()
         return c
 
-    for c in loads[8:]:
-        c.wait()
+    received(wgu, pair_sem.at[1])
+    loads[8].wait()
 
     def rows_of(block):
         rows = jnp.concatenate(
@@ -409,11 +436,13 @@
         )
         at = pl.ds(pl.multiple_of(block * own, own), own)
         scaled = (rows * post[:, at]).astype(bf16)
-        return (
-            jnp.sum(rows * rows, axis=-1, keepdims=True),
-            jnp.dot(scaled, wg[at, :], preferred_element_type=f32),
-            jnp.dot(scaled, wu[at, :], preferred_element_type=f32),
-        )
+        squares = jnp.sum(rows * rows, axis=-1, keepdims=True)
+        if joined:
+            both = jnp.dot(scaled, wgu[at, :], preferred_element_type=f32)
+            return squares, both[:, :inner], both[:, inner:]
+        return squares, *[
+            jnp.dot(scaled, wgu[i, at, :], preferred_element_type=f32) for i in range(2)
+        ]
 
     def arrive(relayed):
         received(gathered.at[0], fan_all.at[relayed])
@@ -452,7 +481,7 @@
         )
 
     def turn(k):
-        return (ep + 1 + k) % ep_count
+        return across(ep_count - 1 - k)
 
     def spread(ref, rows):
         for e in range(ep_count):
@@ -467,11 +496,11 @@
 
     def ret_copy(k):
         return pltpu.make_async_remote_copy(
-            src_ref=ret_send.at[(ep + k) % ep_count],
+            src_ref=ret_send.at[across(k)],
             dst_ref=ret_recv.at[ep],
             send_sem=ret_ss.at[0],
             recv_sem=ret_rs.at[0],
-            device_id={"ep": (ep + k) % ep_count},
+            device_id={"ep": across(k)},
             device_id_type=MESH,
         )
 
@@ -505,7 +534,7 @@
         @pl.when(k < ep_count - 1)
         def _():
             ret_send[e] = total.astype(bf16)
-            ret_copy(k + 1).start()
+            ret_copy(ep_count - 1 - k).start()
 
         @pl.when(k == ep_count - 1)
         def _():
@@ -519,10 +548,8 @@
     returned = jnp.concatenate(
         [ret_recv[e].astype(f32) for e in range(ep_count)], axis=0
     ).astype(bf16)
-    mix = jnp.dot(weight_high, returned, preferred_element_type=f32) + jnp.dot(
-        weight_low, returned, preferred_element_type=f32
-    )
-    out[...] = (residual + mix).astype(bf16)
+    mix = jnp.dot(weight_both, returned, preferred_element_type=f32)
+    out[...] = (residual + (mix[:seqs] + mix[seqs:])).astype(bf16)
 
     received(part_recv, part_ss.at[0])
     received(ret_recv.at[pl.ds(0, ep_count - 1)], pack_ss.at[0])
@@ -577,13 +604,19 @@
         w_down.reshape(w_down.shape[1:]),
     ]
     dma = pltpu.SemaphoreType.DMA
-    pair = (width, 2 * lanes) if lanes % 128 == 0 else (2, width, lanes)
+    def beside(a):
+        rows, columns = a.shape
+        return (rows, 2 * columns) if columns % 128 == 0 else (2, rows, columns)
+
+    gate_up = hbm[13:15]
     scratch = [
-        pltpu.VMEM(pair if a is w_key else a.shape, a.dtype) for a in hbm if a is not w_value
+        pltpu.VMEM(beside(a) if a is w_key or a is gate_up[0] else a.shape, a.dtype)
+        for a in hbm
+        if a is not w_value and a is not gate_up[1]
     ] + [
         pltpu.VMEM((seqs * heads, lanes), f32),
         pltpu.VMEM((seqs * heads, lanes), f32),
-        pltpu.VMEM((seqs * heads, lanes), f32),
+        pltpu.VMEM((seqs, lanes), f32),
         pltpu.VMEM((seqs, lanes), f32),
         pltpu.VMEM((seqs * heads, lanes), f32),
         pltpu.VMEM((2, GROUP, heads, span), f32),
@@ -599,8 +632,8 @@
         pltpu.VMEM((ep_count, cap, own), bf16),
         pltpu.VMEM((ep_count, cap, own), bf16),
         pltpu.VMEM((ep_count, cap, own), f32),
-        dma((11,)),
-        dma((1,)),
+        dma((9,)),
+        dma((2,)),
         dma((3, seqs // GROUP)),
         dma((1,)),
         dma((1,)),

time: 36.9 us -> 35.9 us (0.973)
  Pallas kernels: 36.1 us -> 35.1 us
    pallas_call x1, Pallas kernels: 36.1 us -> 35.1 us  [body(): pl.pallas_call(functools.partial(layer_kernel, ep_count, tp_count), out_s...]
where the time goes in v2:
time: 35.9 us; the launch traced here: 35.7 us
  Pallas kernels  35.1 us (98%)
  local copies, waits for them, and re-layouts  0.62 us (2%)
    pallas_call x1, Pallas kernels, body(): pl.pallas_call(functools.partial(layer_kernel, ep_count, tp_count), out_s...  35.1 us

profile of v2, /device:TPU:0, one launch (start us, length us, event | category | flops | bytes accessed | tf_op | source)
XLA Modules:
  0.0 35.7 jit_solution(6121815233123549191)
XLA Ops:
  0.0 35.1 %shard_map.163 = bf16[32,512]{1,0:T(8,128)(2,1)S(1)} custom-call(s32[32]{0:T(128)} %lengths.1, bf16[32,2048]{1,0:T(8,128)(2,1)} %tokens_h.1, f32[1,2048]{1,0:T(1,128)} %bitcast.16, f32[1,2048]{1,0:T(1,128)} %bitcast.17, bf16[2048,512]{1,0:T(8,128)(2,1)} %wq_h.1, bf16[2048,128]{1,0:T(8,128)(2,1)} %wk_h.1, bf16[2048,128]{1,0:T(8,128)(2,1)} %wv_h.1, ...), custom_call_target="tpu_custom_call" | custom-call | tf_op jit(solution)/shard_map/pallas_call | solution.py:651
  35.1 0.6 %copy.19 = bf16[32,512]{1,0:T(8,128)(2,1)} copy(bf16[32,512]{1,0:T(8,128)(2,1)S(1)} %shard_map.163) | data formatting | bytes 65536

commit v3 on v2

--- a/solution.py
+++ b/solution.py
@@ -400,11 +400,8 @@
             device_id_type=MESH,
         )
 
-    def start_pack(k, c):
+    for k in range(1, ep_count):
         pack_copy(k).start()
-        return c
-
-    lax.fori_loop(1, ep_count, start_pack, 0)
     gathered[tp, ep] = pack_send[ep]
 
     def fan_out(k, c):

time: 35.9 us -> 35.8 us (level)
  no operation moved by 1% of the time
where the time goes in v3:
time: 35.8 us; the launch traced here: 35.6 us
  Pallas kernels  35 us (98%)
  local copies, waits for them, and re-layouts  0.62 us (2%)
    pallas_call x1, Pallas kernels, body(): pl.pallas_call(functools.partial(layer_kernel, ep_count, tp_count), out_s...  35 us

profile of v3, /device:TPU:0, one launch (start us, length us, event | category | flops | bytes accessed | tf_op | source)
XLA Modules:
  0.0 35.6 jit_solution(747720759408338111)
XLA Ops:
  0.0 35.0 %shard_map.163 = bf16[32,512]{1,0:T(8,128)(2,1)S(1)} custom-call(s32[32]{0:T(128)} %lengths.1, bf16[32,2048]{1,0:T(8,128)(2,1)} %tokens_h.1, f32[1,2048]{1,0:T(1,128)} %bitcast.16, f32[1,2048]{1,0:T(1,128)} %bitcast.17, bf16[2048,512]{1,0:T(8,128)(2,1)} %wq_h.1, bf16[2048,128]{1,0:T(8,128)(2,1)} %wk_h.1, bf16[2048,128]{1,0:T(8,128)(2,1)} %wv_h.1, ...), custom_call_target="tpu_custom_call" | custom-call | tf_op jit(solution)/shard_map/pallas_call | solution.py:648
  35.0 0.6 %copy.19 = bf16[32,512]{1,0:T(8,128)(2,1)} copy(bf16[32,512]{1,0:T(8,128)(2,1)S(1)} %shard_map.163) | data formatting | bytes 65536
